TPU v7x, 32 devices: a whole 2x2x4 slice. The times are simulated.
32 devices in a mesh: sp: 16 (over z, y, x), tp: 2 (over core).
Axes of the slice: x: 2, y: 2, z: 4, core: 2. Of those that a mesh axis runs over, the one named last changes fastest.
Arguments:
- hidden_in: bfloat16 [4096, 2048], P('sp'), may hold values from -16 to 16
- query_one: bfloat16 [2048, 512], P(None, 'tp'), may hold values from -0.13258252 to 0.13258252
- query_two: bfloat16 [2048, 512], P(None, 'tp'), may hold values from -0.13258252 to 0.13258252
- key_one: bfloat16 [2048, 512], P(None, 'tp'), may hold values from -0.13258252 to 0.13258252
- key_two: bfloat16 [2048, 512], P(None, 'tp'), may hold values from -0.13258252 to 0.13258252
- value_proj: bfloat16 [2048, 1024], P(None, 'tp'), may hold values from -0.125 to 0.125
- lambdas: float32 [8], P('tp'), may hold values from 0.3 to 0.8
- norm_gain: float32 [128], replicated, may hold values from 0.1 to 1.9
- out_proj: bfloat16 [1024, 2048], P('tp'), may hold values from -0.1875 to 0.1875
Outputs:
- attended: bfloat16 [4096, 2048], P('sp')
All inputs are finite; a program needn't handle non-finite values.
Results may differ from a plain program's by a relative error of at most 0.015.
Values may be sent and summed in bfloat16 or wider, within the bound.
A program may use at most 64 MiB of HBM per device.

v0:
```python
import math
import jax
import jax.numpy as jnp
from jax import lax
from jax.sharding import PartitionSpec as P

epsilon = 1e-06
masked_score = -1e30


def shards(
    hidden_in, query_one, query_two, key_one, key_two, value_proj, lambdas, norm_gain, out_proj
):
    heads_dev = lambdas.shape[0]
    head_qk = query_one.shape[1] // heads_dev
    head_v = value_proj.shape[1] // heads_dev
    width_q = heads_dev * head_qk
    score_scale = 1.75 * head_qk ** (-0.5)
    joined = jnp.concatenate((query_one, query_two, key_one, key_two, value_proj), axis=1)
    projected = jnp.dot(hidden_in, joined, preferred_element_type=jnp.float32).astype(jnp.bfloat16)
    tok_rows = projected.shape[0]
    key_values = projected[:, 2 * width_q :]
    my_index = lax.axis_index("sp")
    offset = my_index * tok_rows
    query_sets = (projected[:, : 2 * width_q],)
    position_sets = (offset + jnp.arange(tok_rows, dtype=jnp.int32),)
    groups = []
    for query_rows, positions in zip(query_sets, position_sets):
        group_rows = query_rows.shape[0]
        query_a = query_rows[:, :width_q].reshape(group_rows, heads_dev, head_qk)
        query_b = query_rows[:, width_q:].reshape(group_rows, heads_dev, head_qk)
        groups.append((query_a, query_b, positions, positions[group_rows - 1]))

    def one_map(queries, keys, value_rows, allowed, running_max, running_sum, accum):
        scores = (
            jnp.einsum("qhd,khd->hqk", queries, keys, preferred_element_type=jnp.float32)
            * score_scale
        )
        scores = jnp.where(allowed[None], scores, masked_score)
        new_max = jnp.maximum(running_max, jnp.max(scores, axis=-1))
        rescale = jnp.exp(running_max - new_max)
        weights = jnp.where(allowed[None], jnp.exp(scores - new_max[..., None]), 0.0)
        new_sum = running_sum * rescale + jnp.sum(weights, axis=-1)
        added = jnp.einsum(
            "hqk,khe->hqe",
            weights.astype(jnp.bfloat16),
            value_rows,
            preferred_element_type=jnp.float32,
        )
        return (new_max, new_sum, accum * rescale[..., None] + added)

    def absorb(group_state, group, kblock, kstart):
        query_a, query_b, positions, last_pos = group
        block_rows = kblock.shape[0]
        k_pos = kstart + jnp.arange(block_rows, dtype=jnp.int32)
        allowed = k_pos[None, :] <= positions[:, None]
        keys_a = kblock[:, :width_q].reshape(block_rows, heads_dev, head_qk)
        keys_b = kblock[:, width_q : 2 * width_q].reshape(block_rows, heads_dev, head_qk)
        value_rows = kblock[:, 2 * width_q :].reshape(block_rows, heads_dev, head_v)
        first_map = one_map(query_a, keys_a, value_rows, allowed, *group_state[:3])
        second_map = one_map(query_b, keys_b, value_rows, allowed, *group_state[3:])
        return first_map + second_map

    group = groups[0]
    group_rows = group[0].shape[0]
    start_max = jnp.full((heads_dev, group_rows), masked_score, jnp.float32)
    start_sum = jnp.zeros((heads_dev, group_rows), jnp.float32)
    start_acc = jnp.zeros((heads_dev, group_rows, head_v), jnp.float32)
    initial_list = [(start_max, start_sum, start_acc, start_max, start_sum, start_acc)]
    initial = tuple(initial_list)
    softmax_state = initial
    kv_piece = lax.all_gather(key_values, "sp", axis=0, tiled=True)
    piece_rows = kv_piece.shape[0]
    block_rows = math.gcd(piece_rows, 512)
    block_count = piece_rows // block_rows
    stacked = kv_piece.reshape(block_count, block_rows, kv_piece.shape[1])

    def absorb_step(carried, blocks_in):
        kblock, block_index = blocks_in
        kstart = block_index * block_rows
        renewed = []
        for group, group_state in zip(groups, carried):
            renewed.append(
                lax.cond(
                    kstart <= group[3],
                    lambda inner, group=group: absorb(inner, group, kblock, kstart),
                    lambda inner: inner,
                    group_state,
                )
            )
        return (tuple(renewed), None)

    softmax_state, _ = lax.scan(
        absorb_step, softmax_state, (stacked, jnp.arange(block_count, dtype=jnp.int32))
    )
    normed_sets = []
    for group_state in softmax_state:
        out_a = group_state[2] / group_state[1][..., None]
        out_b = group_state[5] / group_state[4][..., None]
        mixed_out = out_a - lambdas[:, None, None] * out_b
        scale_rows = lax.rsqrt(jnp.mean(mixed_out * mixed_out, axis=-1, keepdims=True) + epsilon)
        normed = (mixed_out * scale_rows * norm_gain).astype(jnp.bfloat16)
        group_rows = normed.shape[1]
        normed_sets.append(jnp.transpose(normed, (1, 0, 2)).reshape(group_rows, heads_dev * head_v))
    normed_all = normed_sets[0]
    partial_value = jnp.dot(normed_all, out_proj, preferred_element_type=jnp.float32)
    result = lax.psum(partial_value.astype(jnp.bfloat16), "tp")
    return result


def solution(mesh):
    placed = (
        P("sp", None),
        P(None, "tp"),
        P(None, "tp"),
        P(None, "tp"),
        P(None, "tp"),
        P(None, "tp"),
        P("tp"),
        P(),
        P("tp", None),
    )
    return jax.shard_map(
        shards, mesh=mesh, in_specs=placed, out_specs=P("sp", None), check_vma=False
    )
```

profile of v0, /device:TPU:0, one launch (start us, length us, event | category | flops | bytes accessed | tf_op | source)
XLA Modules:
  0.0 254.4 jit_solution(17439998530829736582)
XLA Ops:
  6.5 1.5 constant_dynamic-update-slice_fusion.4
  8.6 0.9 copy-done.4
  9.6 0.6 copy-done.1
  10.3 1.1 copy-done.7
  11.4 1.8 fusion.24
  13.3 0.8 slice.34
  14.2 0.7 slice.27
  14.9 136.6 %all-gather.2.cloned.1.call-done = bf16[4096,1024]{0,1:T(8,128)(2,1)} async-done(((bf16[256,1024]{0,1:T(8,128)(2,1)}), bf16[4096,1024]{0,1:T(8,128)(2,1)}) %all-gather.2.cloned.1.call-update) | async-done | bytes 8388624 | tf_op jit(solution)/shard_map/all_gather | solution.py:72
  151.5 7.4 %copy.26 = bf16[128,8,8,512]{3,2,0,1:T(8,128)(2,1)} copy(bf16[128,8,8,512]{3,2,1,0:T(8,128)(2,1)} %bitcast.57) | data formatting | bytes 16777216 | tf_op jit(solution)/shard_map/reshape | solution.py:76
  159.0 21.9 %while.21 = (s32[]{:T(128)}, f32[4,256]{1,0:T(4,128)S(1)}, f32[4,256]{1,0:T(4,128)S(1)}, f32[4,256,128]{2,1,0:T(8,128)S(1)}, f32[4,256]{1,0:T(4,128)S(1)}, /*ind...) while((s32[]{:T(128)}, f32[4,256]{1,0:T(4,128)S(1)}, ...), condition=%wide.region_7.8_spmd.clone, body=%wide.region_0.7_spmd.clone.sunk | while | flops 416944896 | bytes 23601552 | solution.py:93
  159.1 0.6 dynamic_slice.13
  161.0 6.1 %conditional.3 = ((f32[4,256]{1,0:T(4,128)S(1)}, f32[4,256]{1,0:T(4,128)S(1)}, f32[4,256,128]{2,1,0:T(8,128)S(1)}, f32[4,256]{1,0:T(4,128)S(1)}, f32[4,256]{1,0:T(4,128)S(1)}, /*index=5*/f32[4,256,128]{2,1,0:T(8,128)S(1)})) conditional(s32[]{:T(128)} %convert_element_type.38, (f32[4,256]{1,0:T(4,128)S(1)}, f32[4,256]{1,0:T(4,128)S(1)}, ...), branch_computations={%region_1.1_spmd, %region_2.6_spmd} | conditional | flops 416944896 | bytes 23600196 | solution.py:84
  161.0 1.3 dynamic-slice_bitcast_fusion
  163.0 0.7 fusion.3
  163.8 1.0 fusion.7
  164.9 1.1 convolution_add_fusion
  165.9 1.1 convolution_add_fusion.1
  167.1 0.6 dynamic_slice.13
  169.1 0.6 dynamic_slice.13
  180.9 1.0 copy.18
  182.2 1.2 multiply_reduce_fusion
  183.5 1.7 convolution_convert_fusion
  185.2 60.0 %all-reduce.2.cloned.1.call-done = bf16[256,2048]{1,0:T(8,128)(2,1)} async-done(((bf16[256,2048]{1,0:T(8,128)(2,1)}), bf16[256,2048]{1,0:T(8,128)(2,1)}) %all-reduce.2.cloned.1.call-update) | async-done | bytes 1048592 | tf_op jit(solution)/shard_map/psum | solution.py:107
  245.3 2.3 copy.67
  (64 shorter events, 5.1 us)
Async XLA Ops:
  6.5 177.0 %copy-start = (bf16[512,2048]{1,0:T(8,128)(2,1)S(1)}, bf16[512,2048]{1,0:T(8,128)(2,1)}, u32[]{:S(2)}) copy-start(bf16[512,2048]{1,0:T(8,128)(2,1)} %param.21) | copy-start | bytes 6291460
  6.5 1.7 copy-start.2
  6.5 145.0 %all-gather.2.cloned.1.call-start = ((), (), s32[]{:S(2)}) async-start(), calls=%async_computation | async-start | bytes 8912896 | tf_op jit(solution)/shard_map/all_gather | solution.py:72
  6.5 2.0 copy-start.3
  8.2 1.3 copy-start.4
  8.5 1.7 copy-start.1
  10.2 1.2 copy-start.7
  14.1 231.1 %all-reduce.2.cloned.1.call-start = ((), (), s32[]{:S(2)}) async-start(), calls=%async_computation.1 | async-start | bytes 2097152 | tf_op jit(solution)/shard_map/psum | solution.py:107
  180.9 1.2 copy-start.5
  180.9 2.4 copy-start.6
Sparse Core Ops, SparseCore 0:
  14.3 137.1 all-gather.1
  185.3 59.8 all-reduce.1
where the time goes:
time: 255 us; the launch traced here: 254 us
  waiting for transfers between devices  197 us (77%)
  local copies, waits for them, and re-layouts  23.5 us (9%)
  between operations  13.6 us (5%)
  loops' own time  11.2 us (4%)
  matrix products  6.91 us (3%)
    all_gather x1, waiting for transfers between devices, shards(): kv_piece = lax.all_gather(key_values, 'sp', axis=0, tiled=True)  137 us
    psum x1, waiting for transfers between devices, shards(): result = lax.psum(partial_value.astype(jnp.bfloat16), 'tp')  60 us
    another operation x1, loops' own time, shards(): lax.scan(absorb_step, softmax_state, (stacked, jnp.arange(block_count, dt...  11 us
    reshape x1, local copies, waits for them, and re-layouts, shards(): stacked = kv_piece.reshape(block_count, block_rows, kv_piece.shape[1])  7.41 us
    unnamed x21, local copies, waits for them, and re-layouts  7.03 us
  transfers between devices with their start and end apart: 2, of which 2 were waited for; matrix products, arithmetic and copies ran while one was open for 0% of the time, Pallas kernels for 0%

commit v1 on v0

--- a/solution.py
+++ b/solution.py
@@ -104,7 +104,7 @@
         normed_sets.append(jnp.transpose(normed, (1, 0, 2)).reshape(group_rows, heads_dev * head_v))
     normed_all = normed_sets[0]
     partial_value = jnp.dot(normed_all, out_proj, preferred_element_type=jnp.float32)
-    result = lax.psum(partial_value.astype(jnp.bfloat16), "tp")
+    result = jnp.sum(lax.all_gather(partial_value.astype(jnp.bfloat16), "tp"), axis=0)
     return result
 
 

time: 255 us -> 247 us (0.969)
  waiting for transfers between devices: 197 us -> 188 us
  other arithmetic: 2.53 us -> 5.82 us
    psum x1 -> x0, waiting for transfers between devices: 60 us -> none  [shards(): result = lax.psum(partial_value.astype(jnp.bfloat16), 'tp')]
    all_gather x0 -> x1, waiting for transfers between devices: none -> 51.3 us  [shards(): lax.all_gather(partial_value.astype(jnp.bfloat16), 'tp')]
    reduce_sum x0 -> x1, other arithmetic: none -> 3.31 us  [shards(): jnp.sum(lax.all_gather(partial_value.astype(jnp.bfloat16), 'tp'), axis=0)]
    unnamed x21 -> x20, local copies, waits for them, and re-layouts: 7.03 us -> 4.73 us
where the time goes in v1:
time: 247 us
  waiting for transfers between devices  188 us (76%)
  local copies, waits for them, and re-layouts  21.1 us (9%)
  between operations  13.6 us (6%)
  loops' own time  11.2 us (5%)
  matrix products  6.94 us (3%)
  other arithmetic  5.82 us (2%)
    all_gather x1, waiting for transfers between devices, shards(): kv_piece = lax.all_gather(key_values, 'sp', axis=0, tiled=True)  137 us
    all_gather x1, waiting for transfers between devices, shards(): lax.all_gather(partial_value.astype(jnp.bfloat16), 'tp')  51.3 us
    another operation x1, loops' own time, shards(): lax.scan(absorb_step, softmax_state, (stacked, jnp.arange(block_count, dt...  11 us
    reshape x1, local copies, waits for them, and re-layouts, shards(): stacked = kv_piece.reshape(block_count, block_rows, kv_piece.shape[1])  7.41 us
  transfers between devices with their start and end apart: 2, of which 2 were waited for; matrix products, arithmetic and copies ran while one was open for 0% of the time, Pallas kernels for 0%

profile of v1, /device:TPU:0, one launch (start us, length us, event | category | flops | bytes accessed | tf_op | source)
XLA Modules:
  0.0 246.7 jit_solution(16325013053625180314)
XLA Ops:
  6.5 1.5 constant_dynamic-update-slice_fusion.4
  8.6 0.9 copy-done.4
  9.6 0.6 copy-done.1
  10.3 1.1 copy-done.7
  11.4 1.8 fusion.24
  13.3 0.8 slice.34
  14.2 0.7 slice.27
  14.9 136.6 %all-gather.4.cloned.1.call-done = bf16[4096,1024]{0,1:T(8,128)(2,1)} async-done(((bf16[256,1024]{0,1:T(8,128)(2,1)}), bf16[4096,1024]{0,1:T(8,128)(2,1)}) %all-gather.4.cloned.1.call-update) | async-done | bytes 8388624 | tf_op jit(solution)/shard_map/all_gather | solution.py:72
  151.5 7.4 %copy.26 = bf16[128,8,8,512]{3,2,0,1:T(8,128)(2,1)} copy(bf16[128,8,8,512]{3,2,1,0:T(8,128)(2,1)} %bitcast.58) | data formatting | bytes 16777216 | tf_op jit(solution)/shard_map/reshape | solution.py:76
  159.0 21.9 %while.21 = (s32[]{:T(128)}, f32[4,256]{1,0:T(4,128)S(1)}, f32[4,256]{1,0:T(4,128)S(1)}, f32[4,256,128]{2,1,0:T(8,128)S(1)}, f32[4,256]{1,0:T(4,128)S(1)}, /*ind...) while((s32[]{:T(128)}, f32[4,256]{1,0:T(4,128)S(1)}, ...), condition=%wide.region_7.8_spmd.clone, body=%wide.region_0.7_spmd.clone.sunk | while | flops 416944896 | bytes 23601552 | solution.py:93
  159.1 0.6 dynamic_slice.13
  161.0 6.1 %conditional.3 = ((f32[4,256]{1,0:T(4,128)S(1)}, f32[4,256]{1,0:T(4,128)S(1)}, f32[4,256,128]{2,1,0:T(8,128)S(1)}, f32[4,256]{1,0:T(4,128)S(1)}, f32[4,256]{1,0:T(4,128)S(1)}, /*index=5*/f32[4,256,128]{2,1,0:T(8,128)S(1)})) conditional(s32[]{:T(128)} %convert_element_type.40, (f32[4,256]{1,0:T(4,128)S(1)}, f32[4,256]{1,0:T(4,128)S(1)}, ...), branch_computations={%region_1.1_spmd, %region_2.6_spmd} | conditional | flops 416944896 | bytes 23600196 | solution.py:84
  161.0 1.3 dynamic-slice_bitcast_fusion
  163.0 0.7 fusion.3
  163.8 1.0 fusion.7
  164.9 1.1 convolution_add_fusion
  166.0 1.1 convolution_add_fusion.1
  167.1 0.6 dynamic_slice.13
  169.1 0.6 dynamic_slice.13
  181.0 1.0 copy.18
  182.2 1.2 multiply_reduce_fusion
  183.5 1.7 convolution_convert_fusion
  185.2 51.3 %all-gather.6.cloned.1.call-done = bf16[512,2048]{1,0:T(8,128)(2,1)} async-done(((bf16[256,2048]{1,0:T(8,128)(2,1)}), bf16[512,2048]{1,0:T(8,128)(2,1)}) %all-gather.6.cloned.1.call-update) | async-done | bytes 2097168 | tf_op jit(solution)/shard_map/all_gather | solution.py:107
  236.5 3.3 %reduce_sum.42 = bf16[256,2048]{1,0:T(8,128)(2,1)} reduce(bf16[2,256,2048]{2,1,0:T(8,128)(2,1)} %bitcast.61, bf16[]{:T(256)} %constant.46.clone.1), dimensions={0}, to_apply=%region_9.10 | reduce | flops 524288 | bytes 3145730 | tf_op jit(solution)/shard_map/reduce_sum | solution.py:107
  (64 shorter events, 5.1 us)
Async XLA Ops:
  6.5 177.0 %copy-start = (bf16[512,2048]{1,0:T(8,128)(2,1)S(1)}, bf16[512,2048]{1,0:T(8,128)(2,1)}, u32[]{:S(2)}) copy-start(bf16[512,2048]{1,0:T(8,128)(2,1)} %param.21) | copy-start | bytes 6291460
  6.5 1.7 copy-start.2
  6.5 145.0 %all-gather.4.cloned.1.call-start = ((), (), s32[]{:S(2)}) async-start(), calls=%async_computation | async-start | bytes 8912896 | tf_op jit(solution)/shard_map/all_gather | solution.py:72
  6.5 2.0 copy-start.3
  8.2 1.3 copy-start.4
  8.5 1.7 copy-start.1
  10.2 1.2 copy-start.7
  14.1 222.4 %all-gather.6.cloned.1.call-start = ((), (), s32[]{:S(2)}) async-start(), calls=%async_computation.1 | async-start | bytes 3145728 | tf_op jit(solution)/shard_map/all_gather | solution.py:107
  180.9 1.2 copy-start.5
  180.9 2.4 copy-start.6
Sparse Core Ops, SparseCore 0:
  14.3 137.1 all-gather.3
  185.4 51.1 all-gather.5
